TPU v7x, 32 devices: a whole 2x2x4 slice. The times are simulated.
32 devices in a mesh: fs: 16 (over z, y, x), tp: 2 (over core).
Axes of the slice: x: 2, y: 2, z: 4, core: 2. Of those that a mesh axis runs over, the one named last changes fastest.
Arguments:
- tokens: bfloat16 [6144, 2048], P('fs'), may hold values from -6 to 6
- merged: bfloat16 [6144, 2048], P('fs'), may hold values from -6 to 6
- gain_first: float32 [2048], replicated, may hold values from 0.1 to 1.9
- gate_first: bfloat16 [2048, 2816], P('fs', 'tp'), may hold values from -0.125 to 0.125
- up_first: bfloat16 [2048, 2816], P('fs', 'tp'), may hold values from -0.125 to 0.125
- down_first: bfloat16 [2816, 2048], P('tp', 'fs'), may hold values from -0.21875 to 0.21875
- gain_second: float32 [2048], replicated, may hold values from 0.1 to 1.9
- gate_second: bfloat16 [2048, 2816], P('fs', 'tp'), may hold values from -0.125 to 0.125
- up_second: bfloat16 [2048, 2816], P('fs', 'tp'), may hold values from -0.125 to 0.125
- down_second: bfloat16 [2816, 2048], P('tp', 'fs'), may hold values from -0.21875 to 0.21875
Outputs:
- result: bfloat16 [6144, 2048], P('fs')
All inputs are finite; a program needn't handle non-finite values.
Results may differ from a plain program's by a relative error of at most 0.01.
Values may be sent and summed in bfloat16 or wider, within the bound.
A program may use at most 64 MiB of HBM per device.

v0:
```python
import jax
import jax.numpy as jnp
from jax import lax
from jax.sharding import PartitionSpec as P

EPS = 1e-06


def norm_rows(values, gain):
    scale = lax.rsqrt(jnp.mean(values * values, axis=-1, keepdims=True) + EPS)
    return values * scale * gain


def make_folder(normed, pieces):
    return (
        jnp.dot(normed, pieces[0], preferred_element_type=jnp.float32),
        jnp.dot(normed, pieces[1], preferred_element_type=jnp.float32),
    )


def shards(
    tokens,
    merged,
    gain_first,
    gate_first,
    up_first,
    down_first,
    gain_second,
    gate_second,
    up_second,
    down_second,
):
    normed_first = norm_rows(tokens.astype(jnp.float32), gain_first).astype(jnp.bfloat16)
    gate, up = make_folder(
        normed_first,
        (
            lax.all_gather(gate_first, "fs", axis=0, tiled=True),
            lax.all_gather(up_first, "fs", axis=0, tiled=True),
        ),
    )
    hidden = (jax.nn.silu(gate) * up).astype(jnp.bfloat16)
    down_whole = lax.all_gather(down_first, "fs", axis=1, tiled=True)
    partial_value = jnp.dot(hidden, down_whole, preferred_element_type=jnp.float32)
    first_sum = lax.psum(partial_value.astype(jnp.bfloat16), "tp").astype(jnp.float32)
    middle = tokens.astype(jnp.float32) + merged.astype(jnp.float32) + 0.5 * first_sum
    normed_second = norm_rows(middle, gain_second).astype(jnp.bfloat16)
    gate_two, up_two = make_folder(
        normed_second,
        (
            lax.all_gather(gate_second, "fs", axis=0, tiled=True),
            lax.all_gather(up_second, "fs", axis=0, tiled=True),
        ),
    )
    hidden_two = (jax.nn.silu(gate_two) * up_two).astype(jnp.bfloat16)
    down_two = lax.all_gather(down_second, "fs", axis=1, tiled=True)
    partial_two = jnp.dot(hidden_two, down_two, preferred_element_type=jnp.float32)
    second_sum = lax.psum(partial_two.astype(jnp.bfloat16), "tp").astype(jnp.float32)
    return (middle + 0.5 * second_sum).astype(jnp.bfloat16)


def solution(mesh):
    return jax.shard_map(
        shards,
        mesh=mesh,
        in_specs=(
            P("fs", None),
            P("fs", None),
            P(),
            P("fs", "tp"),
            P("fs", "tp"),
            P("tp", "fs"),
            P(),
            P("fs", "tp"),
            P("fs", "tp"),
            P("tp", "fs"),
        ),
        out_specs=P("fs", None),
        check_vma=False,
    )
```

profile of v0, /device:TPU:0, one launch (start us, length us, event | category | flops | bytes accessed | tf_op | source)
XLA Modules:
  0.0 665.2 jit_solution(4083028435205835512)
XLA Ops:
  6.5 0.0 all-gather.7.cloned.1.call-start
  6.5 0.7 all-gather.7.cloned.1.call-update
  7.3 0.0 all-gather.11.cloned.1.call-start
  7.3 0.7 all-gather.11.cloned.1.call-update
  8.0 0.0 all-gather.9.cloned.1.call-start
  8.1 0.7 all-gather.9.cloned.1.call-update
  8.7 0.0 all-reduce.3.cloned.1.call-start
  8.8 1.8 fusion.1
  10.6 0.0 copy-start
  10.6 0.0 copy-start.4
  10.6 90.9 %all-gather.7.cloned.1.call-done = bf16[2048,1408]{1,0:T(8,128)(2,1)} async-done(((bf16[128,1408]{1,0:T(8,128)(2,1)}), bf16[2048,1408]{1,0:T(8,128)(2,1)}) %all-gather.7.cloned.1.call-update) | async-done | bytes 5767184 | tf_op jit(solution)/shard_map/all_gather | solution.py:37
  101.5 7.1 %fusion.8 = f32[384,1408]{1,0:T(8,128)} fusion(bf16[2048,1408]{1,0:T(8,128)(2,1)} %all-gather.7.cloned.1.call-done, bf16[384,2048]{1,0:T(8,128)(2,1)} %param.10, f32[2048]{0:T(1024)} %param.12, f32[384]{0:T(512)S(1)} %add_rsqrt_fusion.1), kind=kOutput, calls=%fused_computation.16 | convolution fusion | flops 2217738240 | bytes 9512448 | tf_op jit(solution)/shard_map/dot_general | solution.py:16
  108.7 102.6 %all-gather.11.cloned.1.call-done = bf16[1408,2048]{1,0:T(8,128)(2,1)} async-done(((bf16[1408,128]{1,0:T(8,128)(2,1)}), bf16[1408,2048]{1,0:T(8,128)(2,1)}) %all-gather.11.cloned.1.call-update) | async-done | bytes 5767184 | tf_op jit(solution)/shard_map/all_gather | solution.py:42
  211.3 89.7 %all-gather.9.cloned.1.call-done = bf16[2048,1408]{1,0:T(8,128)(2,1)} async-done(((bf16[128,1408]{1,0:T(8,128)(2,1)}), bf16[2048,1408]{1,0:T(8,128)(2,1)}) %all-gather.9.cloned.1.call-update) | async-done | bytes 5767184 | tf_op jit(solution)/shard_map/all_gather | solution.py:38
  300.9 0.0 copy-done
  300.9 0.0 copy-done.4
  300.9 11.2 %convolution_convert_fusion.1 = bf16[384,2048]{1,0:T(8,128)(2,1)} fusion(bf16[1408,2048]{1,0:T(8,128)(2,1)} %all-gather.11.cloned.1.call-done, bf16[2048,1408]{1,0:T(8,128)(2,1)} %all-gather.9.cloned.1.call-done, f32[384,1408]{1,0:T(8,128)} %fusion.8, bf16[384,2048]{1,0:T(8,128)(2,1)S(1)} %copy-done, f32[2048]{0:T(1024)S(1)} %copy-done.4, ...), kind=kOutput, calls=%fused_computation.15 | convolution fusion | flops 4436361216 | bytes 16852480 | tf_op jit(solution)/shard_map/dot_general | solution.py:43
  312.1 0.0 copy-start.1
  312.1 0.0 all-reduce.3.cloned.1.call-update
  312.2 0.0 copy-start.3
  312.2 0.0 all-gather.13.cloned.1.call-start
  312.2 0.5 all-gather.13.cloned.1.call-update
  312.8 0.0 all-gather.15.cloned.1.call-start
  312.8 0.5 all-gather.15.cloned.1.call-update
  313.3 0.0 all-gather.17.cloned.1.call-start
  313.4 0.7 all-gather.17.cloned.1.call-update
  314.1 0.2 all-reduce.5.cloned.1.call-start
  314.3 17.0 %all-reduce.3.cloned.1.call-done = bf16[384,2048]{1,0:T(8,128)(2,1)} async-done(((bf16[384,2048]{1,0:T(8,128)(2,1)}), bf16[384,2048]{1,0:T(8,128)(2,1)}) %all-reduce.3.cloned.1.call-update) | async-done | bytes 1572880 | tf_op jit(solution)/shard_map/psum | solution.py:44
  331.3 0.0 copy-done.1
  331.3 0.0 copy-start.2
  331.3 2.4 multiply_reduce_fusion
  333.8 0.0 copy-done.3
  333.8 0.0 copy-done.2
  333.8 2.2 multiply_convert_fusion
  336.0 87.8 %all-gather.13.cloned.1.call-done = bf16[2048,1408]{1,0:T(8,128)(2,1)} async-done(((bf16[128,1408]{1,0:T(8,128)(2,1)}), bf16[2048,1408]{1,0:T(8,128)(2,1)}) %all-gather.13.cloned.1.call-update) | async-done | bytes 5767184 | tf_op jit(solution)/shard_map/all_gather | solution.py:50
  423.8 7.1 %fusion.12 = f32[384,1408]{1,0:T(8,128)} fusion(bf16[384,2048]{1,0:T(8,128)(2,1)} %multiply_convert_fusion, bf16[2048,1408]{1,0:T(8,128)(2,1)} %all-gather.13.cloned.1.call-done), kind=kOutput, calls=%fused_computation.21 | convolution fusion | flops 2214592512 | bytes 9502720 | tf_op jit(solution)/shard_map/dot_general | solution.py:16
  430.9 82.9 %all-gather.15.cloned.1.call-done = bf16[2048,1408]{1,0:T(8,128)(2,1)} async-done(((bf16[128,1408]{1,0:T(8,128)(2,1)}), bf16[2048,1408]{1,0:T(8,128)(2,1)}) %all-gather.15.cloned.1.call-update) | async-done | bytes 5767184 | tf_op jit(solution)/shard_map/all_gather | solution.py:51
  513.8 109.7 %all-gather.17.cloned.1.call-done = bf16[1408,2048]{1,0:T(8,128)(2,1)} async-done(((bf16[1408,128]{1,0:T(8,128)(2,1)}), bf16[1408,2048]{1,0:T(8,128)(2,1)}) %all-gather.17.cloned.1.call-update) | async-done | bytes 5767184 | tf_op jit(solution)/shard_map/all_gather | solution.py:55
  623.6 11.7 %convolution_convert_fusion = bf16[384,2048]{1,0:T(8,128)(2,1)} fusion(bf16[1408,2048]{1,0:T(8,128)(2,1)} %all-gather.17.cloned.1.call-done, bf16[384,2048]{1,0:T(8,128)(2,1)} %multiply_convert_fusion, bf16[2048,1408]{1,0:T(8,128)(2,1)} %all-gather.15.cloned.1.call-done, f32[384,1408]{1,0:T(8,128)} %fusion.12), kind=kOutput, calls=%fused_computation.14 | convolution fusion | flops 4433215488 | bytes 16842752 | tf_op jit(solution)/shard_map/dot_general | solution.py:56
  635.3 0.0 all-reduce.5.cloned.1.call-update
  635.3 18.7 %all-reduce.5.cloned.1.call-done = bf16[384,2048]{1,0:T(8,128)(2,1)} async-done(((bf16[384,2048]{1,0:T(8,128)(2,1)}), bf16[384,2048]{1,0:T(8,128)(2,1)}) %all-reduce.5.cloned.1.call-update) | async-done | bytes 1572880 | tf_op jit(solution)/shard_map/psum | solution.py:57
  654.0 4.3 add_convert_fusion
  (2 shorter events, 0.0 us)
Async XLA Ops:
  6.5 95.0 %all-gather.7.cloned.1.call-start = ((), (), s32[]{:S(2)}) async-start(), calls=%async_computation | async-start | bytes 6127616 | tf_op jit(solution)/shard_map/all_gather | solution.py:37
  7.3 204.0 %all-gather.11.cloned.1.call-start = ((), (), s32[]{:S(2)}) async-start(), calls=%async_computation.2 | async-start | bytes 6127616 | tf_op jit(solution)/shard_map/all_gather | solution.py:42
  8.0 292.9 %all-gather.9.cloned.1.call-start = ((), (), s32[]{:S(2)}) async-start(), calls=%async_computation.1 | async-start | bytes 6127616 | tf_op jit(solution)/shard_map/all_gather | solution.py:38
  8.7 322.6 %all-reduce.3.cloned.1.call-start = ((), (), s32[]{:S(2)}) async-start(), calls=%async_computation.3 | async-start | bytes 3145728 | tf_op jit(solution)/shard_map/psum | solution.py:44
  10.6 290.3 %copy-start = (bf16[384,2048]{1,0:T(8,128)(2,1)S(1)}, bf16[384,2048]{1,0:T(8,128)(2,1)}, u32[]{:S(2)}) copy-start(bf16[384,2048]{1,0:T(8,128)(2,1)} %param.10) | copy-start | bytes 4718596
  10.6 290.3 %copy-start.4 = (f32[2048]{0:T(1024)S(1)}, f32[2048]{0:T(1024)}, u32[]{:S(2)}) copy-start(f32[2048]{0:T(1024)} %param.12) | copy-start | bytes 24580
  312.1 19.2 %copy-start.1 = (bf16[384,2048]{1,0:T(8,128)(2,1)S(1)}, bf16[384,2048]{1,0:T(8,128)(2,1)}, u32[]{:S(2)}) copy-start(bf16[384,2048]{1,0:T(8,128)(2,1)} %param.11) | copy-start | bytes 4718596
  312.2 21.6 %copy-start.3 = (f32[2048]{0:T(1024)S(1)}, f32[2048]{0:T(1024)}, u32[]{:S(2)}) copy-start(f32[2048]{0:T(1024)} %param.16) | copy-start | bytes 24580
  312.2 111.7 %all-gather.13.cloned.1.call-start = ((), (), s32[]{:S(2)}) async-start(), calls=%async_computation.4 | async-start | bytes 6127616 | tf_op jit(solution)/shard_map/all_gather | solution.py:50
  312.8 201.1 %all-gather.15.cloned.1.call-start = ((), (), s32[]{:S(2)}) async-start(), calls=%async_computation.5 | async-start | bytes 6127616 | tf_op jit(solution)/shard_map/all_gather | solution.py:51
  313.3 310.2 %all-gather.17.cloned.1.call-start = ((), (), s32[]{:S(2)}) async-start(), calls=%async_computation.6 | async-start | bytes 6127616 | tf_op jit(solution)/shard_map/all_gather | solution.py:55
  314.1 340.0 %all-reduce.5.cloned.1.call-start = ((), (), s32[]{:S(2)}) async-start(), calls=%async_computation.7 | async-start | bytes 3145728 | tf_op jit(solution)/shard_map/psum | solution.py:57
  331.3 2.4 copy-start.2
Sparse Core Ops, SparseCore 0:
  10.0 91.4 all-gather.6
  104.2 106.9 all-gather.10
  213.9 86.9 all-gather.8
  312.3 19.0 all-reduce.2
  333.9 89.9 all-gather.12
  426.4 87.4 all-gather.14
  516.5 106.9 all-gather.16
  635.4 18.5 all-reduce.4
where the time goes:
time: 665 us
  waiting for transfers between devices  603 us (91%)
  matrix products  37.1 us (6%)
  between operations  13.5 us (2%)
  other arithmetic  10.8 us (2%)
    all_gather x1, waiting for transfers between devices, shards(): down_two = lax.all_gather(down_second, 'fs', axis=1, tiled=True)  110 us
    all_gather x1, waiting for transfers between devices, shards(): down_whole = lax.all_gather(down_first, 'fs', axis=1, tiled=True)  103 us
    all_gather x1, waiting for transfers between devices, shards(): lax.all_gather(gate_first, 'fs', axis=0, tiled=True)  90.9 us
    all_gather x1, waiting for transfers between devices, shards(): lax.all_gather(up_first, 'fs', axis=0, tiled=True)  89.7 us
    all_gather x1, waiting for transfers between devices, shards(): lax.all_gather(gate_second, 'fs', axis=0, tiled=True)  87.8 us
    all_gather x1, waiting for transfers between devices, shards(): lax.all_gather(up_second, 'fs', axis=0, tiled=True)  82.9 us
    psum x1, waiting for transfers between devices, shards(): lax.psum(partial_two.astype(jnp.bfloat16), 'tp').astype(jnp.float32)  18.7 us
    psum x1, waiting for transfers between devices, shards(): lax.psum(partial_value.astype(jnp.bfloat16), 'tp').astype(jnp.float32)  17 us
  transfers between devices with their start and end apart: 8, of which 8 were waited for; matrix products, arithmetic and copies ran while one was open for 3% of the time, Pallas kernels for 0%

commit v1 on v0

--- a/solution.py
+++ b/solution.py
@@ -52,7 +52,12 @@
         ),
     )
     hidden_two = (jax.nn.silu(gate_two) * up_two).astype(jnp.bfloat16)
-    down_two = lax.all_gather(down_second, "fs", axis=1, tiled=True)
+    ring = [down_second]
+    for hop in range(15):
+        ring.append(lax.ppermute(ring[-1], "fs", [(dev, (dev + 1) % 16) for dev in range(16)]))
+    down_two = jnp.roll(
+        jnp.concatenate(ring[::-1], axis=1), (lax.axis_index("fs") + 1) * ring[0].shape[1], axis=1
+    )
     partial_two = jnp.dot(hidden_two, down_two, preferred_element_type=jnp.float32)
     second_sum = lax.psum(partial_two.astype(jnp.bfloat16), "tp").astype(jnp.float32)
     return (middle + 0.5 * second_sum).astype(jnp.bfloat16)

time: 665 us -> 641 us (0.964)
  waiting for transfers between devices: 603 us -> 533 us
  local copies, waits for them, and re-layouts: 0.02 us -> 43.6 us
    ppermute x0 -> x15, waiting for transfers between devices: none -> 231 us  [shards(): lax.ppermute(ring[-1], 'fs', [(dev, (dev + 1) % 16) for dev in range(16)])]
    all_gather x1 -> x0, waiting for transfers between devices: 110 us -> none  [shards(): down_two = lax.all_gather(down_second, 'fs', axis=1, tiled=True)]
    all_gather x1, waiting for transfers between devices: 87.8 us -> 0.01 us  [shards(): lax.all_gather(gate_second, 'fs', axis=0, tiled=True)]
    all_gather x1, waiting for transfers between devices: 82.9 us -> 0.01 us  [shards(): lax.all_gather(up_second, 'fs', axis=0, tiled=True)]
    unnamed x10 -> x87, local copies, waits for them, and re-layouts: 0.02 us -> 42.8 us
    psum x1, waiting for transfers between devices: 17 us -> 0.01 us  [shards(): lax.psum(partial_value.astype(jnp.bfloat16), 'tp').astype(jnp.float32)]
  transfers between devices with their start and end apart: 8 -> 22, of which waited for: 8 -> 19; matrix products, arithmetic and copies ran while one was open for 3% -> 9% of each run, Pallas kernels for 0% -> 0%
where the time goes in v1:
time: 641 us; the launch traced here: 640 us
  waiting for transfers between devices  533 us (83%)
  local copies, waits for them, and re-layouts  43.6 us (7%)
  matrix products  37.2 us (6%)
  between operations  13.6 us (2%)
  other arithmetic  10.8 us (2%)
    ppermute x15, waiting for transfers between devices, shards(): lax.ppermute(ring[-1], 'fs', [(dev, (dev + 1) % 16) for dev in range(16)])  231 us
    all_gather x1, waiting for transfers between devices, shards(): down_whole = lax.all_gather(down_first, 'fs', axis=1, tiled=True)  103 us
    all_gather x1, waiting for transfers between devices, shards(): lax.all_gather(gate_first, 'fs', axis=0, tiled=True)  90.9 us
    all_gather x1, waiting for transfers between devices, shards(): lax.all_gather(up_first, 'fs', axis=0, tiled=True)  89.7 us
    unnamed x87, local copies, waits for them, and re-layouts  42.8 us
    psum x1, waiting for transfers between devices, shards(): lax.psum(partial_two.astype(jnp.bfloat16), 'tp').astype(jnp.float32)  16.4 us
    dot_general x2, matrix products, make_folder(): jnp.dot(normed, pieces[0], preferred_element_type=jnp.float32)  14.2 us
  transfers between devices with their start and end apart: 22, of which 19 were waited for; matrix products, arithmetic and copies ran while one was open for 9% of the time, Pallas kernels for 0%

profile of v1, /device:TPU:0, one launch (start us, length us, event | category | flops | bytes accessed | tf_op | source)
XLA Modules:
  0.0 640.3 jit_solution(17723672053163148268)
XLA Ops:
  8.8 1.8 fusion.3
  10.6 90.9 %all-gather.6.cloned.1.call-done = bf16[2048,1408]{1,0:T(8,128)(2,1)} async-done(((bf16[128,1408]{1,0:T(8,128)(2,1)}), bf16[2048,1408]{1,0:T(8,128)(2,1)}) %all-gather.6.cloned.1.call-update) | async-done | bytes 5767184 | tf_op jit(solution)/shard_map/all_gather | solution.py:37
  101.5 7.1 %fusion.13 = f32[384,1408]{1,0:T(8,128)} fusion(bf16[2048,1408]{1,0:T(8,128)(2,1)} %all-gather.6.cloned.1.call-done, bf16[384,2048]{1,0:T(8,128)(2,1)} %param.10, f32[2048]{0:T(1024)} %param.12, f32[384]{0:T(512)S(1)} %add_rsqrt_fusion.1), kind=kOutput, calls=%fused_computation.18 | convolution fusion | flops 2217738240 | bytes 9512448 | tf_op jit(solution)/shard_map/dot_general | solution.py:16
  108.6 102.6 %all-gather.10.cloned.1.call-done = bf16[1408,2048]{1,0:T(8,128)(2,1)} async-done(((bf16[1408,128]{1,0:T(8,128)(2,1)}), bf16[1408,2048]{1,0:T(8,128)(2,1)}) %all-gather.10.cloned.1.call-update) | async-done | bytes 5767184 | tf_op jit(solution)/shard_map/all_gather | solution.py:42
  211.3 89.7 %all-gather.8.cloned.1.call-done = bf16[2048,1408]{1,0:T(8,128)(2,1)} async-done(((bf16[128,1408]{1,0:T(8,128)(2,1)}), bf16[2048,1408]{1,0:T(8,128)(2,1)}) %all-gather.8.cloned.1.call-update) | async-done | bytes 5767184 | tf_op jit(solution)/shard_map/all_gather | solution.py:38
  300.9 11.2 %convolution_convert_fusion = bf16[384,2048]{1,0:T(8,128)(2,1)} fusion(bf16[1408,2048]{1,0:T(8,128)(2,1)} %all-gather.10.cloned.1.call-done, bf16[2048,1408]{1,0:T(8,128)(2,1)} %all-gather.8.cloned.1.call-done, f32[384,1408]{1,0:T(8,128)} %fusion.13, bf16[384,2048]{1,0:T(8,128)(2,1)S(1)} %copy-done, f32[2048]{0:T(1024)S(1)} %copy-done.27, ...), kind=kOutput, calls=%fused_computation.17 | convolution fusion | flops 4436361216 | bytes 16852480 | tf_op jit(solution)/shard_map/dot_general | solution.py:43
  312.8 1.5 collective-permute-start
  314.3 11.2 %collective-permute-done = bf16[1408,128]{1,0:T(8,128)(2,1)S(1)} collective-permute-done((bf16[1408,128]{1,0:T(8,128)(2,1)S(1)}, bf16[1408,128]{1,0:T(8,128)(2,1)S(1)}, u32[]{:S(2)}, u32[]{:S(2)}) %collective-permute-start) | collective-permute-done | bytes 360480 | tf_op jit(solution)/shard_map/ppermute | solution.py:57
  325.5 11.8 %collective-permute-done.1 = bf16[1408,128]{1,0:T(8,128)(2,1)S(1)} collective-permute-done((bf16[1408,128]{1,0:T(8,128)(2,1)S(1)}, bf16[1408,128]{1,0:T(8,128)(2,1)S(1)}, u32[]{:S(2)}, u32[]{:S(2)}) %collective-permute-start.1) | collective-permute-done | bytes 360480 | tf_op jit(solution)/shard_map/ppermute | solution.py:57
  337.3 11.1 %collective-permute-done.2 = bf16[1408,128]{1,0:T(8,128)(2,1)S(1)} collective-permute-done((bf16[1408,128]{1,0:T(8,128)(2,1)S(1)}, bf16[1408,128]{1,0:T(8,128)(2,1)S(1)}, u32[]{:S(2)}, u32[]{:S(2)}) %collective-permute-start.2) | collective-permute-done | bytes 360480 | tf_op jit(solution)/shard_map/ppermute | solution.py:57
  348.4 17.2 %collective-permute-done.3 = bf16[1408,128]{1,0:T(8,128)(2,1)S(1)} collective-permute-done((bf16[1408,128]{1,0:T(8,128)(2,1)S(1)}, bf16[1408,128]{1,0:T(8,128)(2,1)S(1)}, u32[]{:S(2)}, u32[]{:S(2)}) %collective-permute-start.3) | collective-permute-done | bytes 360480 | tf_op jit(solution)/shard_map/ppermute | solution.py:57
  365.7 20.4 %collective-permute-done.4 = bf16[1408,128]{1,0:T(8,128)(2,1)S(1)} collective-permute-done((bf16[1408,128]{1,0:T(8,128)(2,1)S(1)}, bf16[1408,128]{1,0:T(8,128)(2,1)S(1)}, u32[]{:S(2)}, u32[]{:S(2)}) %collective-permute-start.4) | collective-permute-done | bytes 360480 | tf_op jit(solution)/shard_map/ppermute | solution.py:57
  386.0 0.8 copy-done.12
  386.8 14.2 %collective-permute-done.5 = bf16[1408,128]{1,0:T(8,128)(2,1)S(1)} collective-permute-done((bf16[1408,128]{1,0:T(8,128)(2,1)S(1)}, bf16[1408,128]{1,0:T(8,128)(2,1)S(1)}, u32[]{:S(2)}, u32[]{:S(2)}) %collective-permute-start.5) | collective-permute-done | bytes 360480 | tf_op jit(solution)/shard_map/ppermute | solution.py:57
  401.0 0.7 copy-done.14
  401.8 21.5 %collective-permute-done.6 = bf16[1408,128]{1,0:T(8,128)(2,1)S(1)} collective-permute-done((bf16[1408,128]{1,0:T(8,128)(2,1)S(1)}, bf16[1408,128]{1,0:T(8,128)(2,1)S(1)}, u32[]{:S(2)}, u32[]{:S(2)}) %collective-permute-start.6) | collective-permute-done | bytes 360480 | tf_op jit(solution)/shard_map/ppermute | solution.py:57
  424.0 21.2 %collective-permute-done.7 = bf16[1408,128]{1,0:T(8,128)(2,1)S(1)} collective-permute-done((bf16[1408,128]{1,0:T(8,128)(2,1)S(1)}, bf16[1408,128]{1,0:T(8,128)(2,1)S(1)}, u32[]{:S(2)}, u32[]{:S(2)}) %collective-permute-start.7) | collective-permute-done | bytes 360480 | tf_op jit(solution)/shard_map/ppermute | solution.py:57
  446.0 13.5 %collective-permute-done.8 = bf16[1408,128]{1,0:T(8,128)(2,1)S(1)} collective-permute-done((bf16[1408,128]{1,0:T(8,128)(2,1)S(1)}, bf16[1408,128]{1,0:T(8,128)(2,1)S(1)}, u32[]{:S(2)}, u32[]{:S(2)}) %collective-permute-start.8) | collective-permute-done | bytes 360480 | tf_op jit(solution)/shard_map/ppermute | solution.py:57
  459.5 0.8 copy-done.20
  460.3 12.4 %collective-permute-done.9 = bf16[1408,128]{1,0:T(8,128)(2,1)S(1)} collective-permute-done((bf16[1408,128]{1,0:T(8,128)(2,1)S(1)}, bf16[1408,128]{1,0:T(8,128)(2,1)S(1)}, u32[]{:S(2)}, u32[]{:S(2)}) %collective-permute-start.9) | collective-permute-done | bytes 360480 | tf_op jit(solution)/shard_map/ppermute | solution.py:57
  472.7 0.7 copy-done.22
  473.4 11.6 %collective-permute-done.10 = bf16[1408,128]{1,0:T(8,128)(2,1)} collective-permute-done((bf16[1408,128]{1,0:T(8,128)(2,1)S(1)}, bf16[1408,128]{1,0:T(8,128)(2,1)}, u32[]{:S(2)}, u32[]{:S(2)}) %collective-permute-start.10) | collective-permute-done | bytes 360480 | tf_op jit(solution)/shard_map/ppermute | solution.py:57
  485.1 11.3 %collective-permute-done.11 = bf16[1408,128]{1,0:T(8,128)(2,1)} collective-permute-done((bf16[1408,128]{1,0:T(8,128)(2,1)}, bf16[1408,128]{1,0:T(8,128)(2,1)}, u32[]{:S(2)}, u32[]{:S(2)}) %collective-permute-start.11) | collective-permute-done | bytes 360480 | tf_op jit(solution)/shard_map/ppermute | solution.py:57
  496.4 19.3 %collective-permute-done.12 = bf16[1408,128]{1,0:T(8,128)(2,1)S(1)} collective-permute-done((bf16[1408,128]{1,0:T(8,128)(2,1)}, bf16[1408,128]{1,0:T(8,128)(2,1)S(1)}, u32[]{:S(2)}, u32[]{:S(2)}) %collective-permute-start.12) | collective-permute-done | bytes 360480 | tf_op jit(solution)/shard_map/ppermute | solution.py:57
  516.4 19.8 %collective-permute-done.13 = bf16[1408,128]{1,0:T(8,128)(2,1)} collective-permute-done((bf16[1408,128]{1,0:T(8,128)(2,1)S(1)}, bf16[1408,128]{1,0:T(8,128)(2,1)}, u32[]{:S(2)}, u32[]{:S(2)}) %collective-permute-start.13) | collective-permute-done | bytes 360480 | tf_op jit(solution)/shard_map/ppermute | solution.py:57
  536.3 14.5 %collective-permute-done.14 = bf16[1408,128]{1,0:T(8,128)(2,1)} collective-permute-done((bf16[1408,128]{1,0:T(8,128)(2,1)}, bf16[1408,128]{1,0:T(8,128)(2,1)}, u32[]{:S(2)}, u32[]{:S(2)}) %collective-permute-start.14) | collective-permute-done | bytes 360480 | tf_op jit(solution)/shard_map/ppermute | solution.py:57
  550.8 1.9 constant_dynamic-update-slice_fusion.31
  552.7 1.8 constant_dynamic-update-slice_fusion.30
  554.5 1.9 constant_dynamic-update-slice_fusion.29
  556.3 1.8 constant_dynamic-update-slice_fusion.28
  558.1 1.8 constant_dynamic-update-slice_fusion.27
  559.9 1.9 constant_dynamic-update-slice_fusion.26
  561.8 1.8 constant_dynamic-update-slice_fusion.25
  563.6 1.8 constant_dynamic-update-slice_fusion.24
  565.5 0.8 constant_dynamic-update-slice_fusion.23
  566.3 0.8 constant_dynamic-update-slice_fusion.22
  567.1 0.8 constant_dynamic-update-slice_fusion.21
  568.0 0.8 constant_dynamic-update-slice_fusion.20
  568.8 0.8 constant_dynamic-update-slice_fusion.19
  569.6 0.8 constant_dynamic-update-slice_fusion.18
  570.4 0.8 constant_dynamic-update-slice_fusion.17
  571.2 0.8 constant_dynamic-update-slice_fusion.16
  572.0 2.0 constant_dynamic-update-slice_fusion.15
  574.0 1.8 constant_dynamic-update-slice_fusion.14
  575.8 0.8 constant_dynamic-update-slice_fusion.13
  576.6 1.8 constant_dynamic-update-slice_fusion.12
  578.4 1.8 constant_dynamic-update-slice_fusion.11
  580.2 0.8 constant_dynamic-update-slice_fusion.10
  581.0 0.8 constant_dynamic-update-slice_fusion.9
  581.8 0.8 constant_dynamic-update-slice_fusion.8
  582.6 0.8 constant_dynamic-update-slice_fusion.7
  583.4 0.8 constant_dynamic-update-slice_fusion.6
  584.2 0.8 constant_dynamic-update-slice_fusion.5
  585.1 0.8 constant_dynamic-update-slice_fusion.4
  585.9 0.8 constant_dynamic-update-slice_fusion.3
  586.7 0.8 constant_dynamic-update-slice_fusion.2
  587.5 0.8 constant_dynamic-update-slice_fusion.1
  588.3 0.8 constant_dynamic-update-slice_fusion
  589.2 2.4 multiply_reduce_fusion
  591.6 2.2 multiply_convert_fusion
  593.8 7.1 %fusion.18 = f32[384,1408]{1,0:T(8,128)} fusion(bf16[384,2048]{1,0:T(8,128)(2,1)} %multiply_convert_fusion, bf16[2048,1408]{1,0:T(8,128)(2,1)} %all-gather.12.cloned.1.call-done), kind=kOutput, calls=%fused_computation.56 | convolution fusion | flops 2214592512 | bytes 9502720 | tf_op jit(solution)/shard_map/dot_general | solution.py:16
  601.0 11.8 %fusion.8 = bf16[384,2048]{1,0:T(8,128)(2,1)} fusion(bf16[1408,4096]{1,0:T(8,128)(2,1)} %constant_dynamic-update-slice_fusion, s32[]{:T(128)S(6)} %select_n.14, bf16[384,2048]{1,0:T(8,128)(2,1)} %multiply_convert_fusion, bf16[2048,1408]{1,0:T(8,128)(2,1)} %all-gather.14.cloned.1.call-done, f32[384,1408]{1,0:T(8,128)} %fusion.18), kind=kOutput, calls=%fused_computation.16 | convolution fusion | flops 4433215488 | bytes 16842756 | tf_op jit(solution)/shard_map/dot_general | solution.py:61
  612.7 16.4 %all-reduce.5.cloned.1.call-done = bf16[384,2048]{1,0:T(8,128)(2,1)} async-done(((bf16[384,2048]{1,0:T(8,128)(2,1)}), bf16[384,2048]{1,0:T(8,128)(2,1)}) %all-reduce.5.cloned.1.call-update) | async-done | bytes 1572880 | tf_op jit(solution)/shard_map/psum | solution.py:62
  629.1 4.3 add_convert_fusion
  (85 shorter events, 5.3 us)
Async XLA Ops:
  6.5 95.0 %all-gather.6.cloned.1.call-start = ((), (), s32[]{:S(2)}) async-start(), calls=%async_computation | async-start | bytes 6127616 | tf_op jit(solution)/shard_map/all_gather | solution.py:37
  7.3 204.0 %all-gather.10.cloned.1.call-start = ((), (), s32[]{:S(2)}) async-start(), calls=%async_computation.2 | async-start | bytes 6127616 | tf_op jit(solution)/shard_map/all_gather | solution.py:42
  8.0 292.9 %all-gather.8.cloned.1.call-start = ((), (), s32[]{:S(2)}) async-start(), calls=%async_computation.1 | async-start | bytes 6127616 | tf_op jit(solution)/shard_map/all_gather | solution.py:38
  8.7 580.4 %all-reduce.3.cloned.1.call-start = ((), (), s32[]{:S(2)}) async-start(), calls=%async_computation.3 | async-start | bytes 3145728 | tf_op jit(solution)/shard_map/psum | solution.py:44
  10.6 290.3 %copy-start = (bf16[384,2048]{1,0:T(8,128)(2,1)S(1)}, bf16[384,2048]{1,0:T(8,128)(2,1)}, u32[]{:S(2)}) copy-start(bf16[384,2048]{1,0:T(8,128)(2,1)} %param.10) | copy-start | bytes 4718596
  10.6 290.3 %copy-start.27 = (f32[2048]{0:T(1024)S(1)}, f32[2048]{0:T(1024)}, u32[]{:S(2)}) copy-start(f32[2048]{0:T(1024)} %param.12) | copy-start | bytes 24580
  108.6 204.1 %copy-start.3 = (bf16[1408,128]{1,0:T(8,128)(2,1)S(1)}, bf16[1408,128]{1,0:T(8,128)(2,1)}, u32[]{:S(2)}) copy-start(bf16[1408,128]{1,0:T(8,128)(2,1)} %param.19) | copy-start | bytes 1081348
  312.1 281.7 %all-gather.12.cloned.1.call-start = ((), (), s32[]{:S(2)}) async-start(), calls=%async_computation.4 | async-start | bytes 6127616 | tf_op jit(solution)/shard_map/all_gather | solution.py:50
  312.7 288.2 %all-gather.14.cloned.1.call-start = ((), (), s32[]{:S(2)}) async-start(), calls=%async_computation.5 | async-start | bytes 6127616 | tf_op jit(solution)/shard_map/all_gather | solution.py:51
  312.8 12.7 %collective-permute-start = (bf16[1408,128]{1,0:T(8,128)(2,1)S(1)}, bf16[1408,128]{1,0:T(8,128)(2,1)S(1)}, u32[]{:S(2)}, u32[]{:S(2)}) collective-permute-start(bf16[1408,128]{1,0:T(8,128)(2,1)S(1)} %copy-done.3), channel_id=1, source_target_pairs={{0,2},{2,4},{4,6},{6,8},{8,10},{10,12},{12,14},{14,16},{16,18},{18... | collective-permute-start | bytes 1081352 | tf_op jit(solution)/shard_map/ppermute | solution.py:57
  325.5 245.7 %copy-start.4 = (bf16[1408,128]{1,0:T(8,128)(2,1)}, bf16[1408,128]{1,0:T(8,128)(2,1)S(1)}, u32[]{:S(2)}) copy-start(bf16[1408,128]{1,0:T(8,128)(2,1)S(1)} %collective-permute-done) | copy-start | bytes 1081348
  325.5 11.8 %collective-permute-start.1 = (bf16[1408,128]{1,0:T(8,128)(2,1)S(1)}, bf16[1408,128]{1,0:T(8,128)(2,1)S(1)}, u32[]{:S(2)}, u32[]{:S(2)}) collective-permute-start(bf16[1408,128]{1,0:T(8,128)(2,1)S(1)} %collective-permute-done), channel_id=1, source_target_pairs={{0,2},{2,4},{4,6},{6,8},{8,10},{10,12},{12,14},{14,16},{16,18},{18... | collective-permute-start | bytes 1081352 | tf_op jit(solution)/shard_map/ppermute | solution.py:57
  337.3 233.9 %copy-start.6 = (bf16[1408,128]{1,0:T(8,128)(2,1)}, bf16[1408,128]{1,0:T(8,128)(2,1)S(1)}, u32[]{:S(2)}) copy-start(bf16[1408,128]{1,0:T(8,128)(2,1)S(1)} %collective-permute-done.1) | copy-start | bytes 1081348
  337.3 11.1 %collective-permute-start.2 = (bf16[1408,128]{1,0:T(8,128)(2,1)S(1)}, bf16[1408,128]{1,0:T(8,128)(2,1)S(1)}, u32[]{:S(2)}, u32[]{:S(2)}) collective-permute-start(bf16[1408,128]{1,0:T(8,128)(2,1)S(1)} %collective-permute-done.1), channel_id=1, source_target_pairs={{0,2},{2,4},{4,6},{6,8},{8,10},{10,12},{12,14},{14,16},{16,18},{18... | collective-permute-start | bytes 1081352 | tf_op jit(solution)/shard_map/ppermute | solution.py:57
  348.4 222.8 %copy-start.8 = (bf16[1408,128]{1,0:T(8,128)(2,1)}, bf16[1408,128]{1,0:T(8,128)(2,1)S(1)}, u32[]{:S(2)}) copy-start(bf16[1408,128]{1,0:T(8,128)(2,1)S(1)} %collective-permute-done.2) | copy-start | bytes 1081348
  348.4 17.2 %collective-permute-start.3 = (bf16[1408,128]{1,0:T(8,128)(2,1)S(1)}, bf16[1408,128]{1,0:T(8,128)(2,1)S(1)}, u32[]{:S(2)}, u32[]{:S(2)}) collective-permute-start(bf16[1408,128]{1,0:T(8,128)(2,1)S(1)} %collective-permute-done.2), channel_id=1, source_target_pairs={{0,2},{2,4},{4,6},{6,8},{8,10},{10,12},{12,14},{14,16},{16,18},{18... | collective-permute-start | bytes 1081352 | tf_op jit(solution)/shard_map/ppermute | solution.py:57
  365.7 205.6 %copy-start.10 = (bf16[1408,128]{1,0:T(8,128)(2,1)}, bf16[1408,128]{1,0:T(8,128)(2,1)S(1)}, u32[]{:S(2)}) copy-start(bf16[1408,128]{1,0:T(8,128)(2,1)S(1)} %collective-permute-done.3) | copy-start | bytes 1081348
  365.7 20.4 %collective-permute-start.4 = (bf16[1408,128]{1,0:T(8,128)(2,1)S(1)}, bf16[1408,128]{1,0:T(8,128)(2,1)S(1)}, u32[]{:S(2)}, u32[]{:S(2)}) collective-permute-start(bf16[1408,128]{1,0:T(8,128)(2,1)S(1)} %collective-permute-done.3), channel_id=1, source_target_pairs={{0,2},{2,4},{4,6},{6,8},{8,10},{10,12},{12,14},{14,16},{16,18},{18... | collective-permute-start | bytes 1081352 | tf_op jit(solution)/shard_map/ppermute | solution.py:57
  386.0 0.8 copy-start.12
  386.8 14.2 %collective-permute-start.5 = (bf16[1408,128]{1,0:T(8,128)(2,1)S(1)}, bf16[1408,128]{1,0:T(8,128)(2,1)S(1)}, u32[]{:S(2)}, u32[]{:S(2)}) collective-permute-start(bf16[1408,128]{1,0:T(8,128)(2,1)S(1)} %collective-permute-done.4), channel_id=1, source_target_pairs={{0,2},{2,4},{4,6},{6,8},{8,10},{10,12},{12,14},{14,16},{16,18},{18... | collective-permute-start | bytes 1081352 | tf_op jit(solution)/shard_map/ppermute | solution.py:57
  401.0 0.8 copy-start.14
  401.8 21.5 %collective-permute-start.6 = (bf16[1408,128]{1,0:T(8,128)(2,1)S(1)}, bf16[1408,128]{1,0:T(8,128)(2,1)S(1)}, u32[]{:S(2)}, u32[]{:S(2)}) collective-permute-start(bf16[1408,128]{1,0:T(8,128)(2,1)S(1)} %collective-permute-done.5), channel_id=1, source_target_pairs={{0,2},{2,4},{4,6},{6,8},{8,10},{10,12},{12,14},{14,16},{16,18},{18... | collective-permute-start | bytes 1081352 | tf_op jit(solution)/shard_map/ppermute | solution.py:57
  423.3 0.7 copy-start.16
  424.0 21.3 %collective-permute-start.7 = (bf16[1408,128]{1,0:T(8,128)(2,1)S(1)}, bf16[1408,128]{1,0:T(8,128)(2,1)S(1)}, u32[]{:S(2)}, u32[]{:S(2)}) collective-permute-start(bf16[1408,128]{1,0:T(8,128)(2,1)S(1)} %collective-permute-done.6), channel_id=1, source_target_pairs={{0,2},{2,4},{4,6},{6,8},{8,10},{10,12},{12,14},{14,16},{16,18},{18... | collective-permute-start | bytes 1081352 | tf_op jit(solution)/shard_map/ppermute | solution.py:57
  445.2 0.7 copy-start.18
  446.0 13.5 %collective-permute-start.8 = (bf16[1408,128]{1,0:T(8,128)(2,1)S(1)}, bf16[1408,128]{1,0:T(8,128)(2,1)S(1)}, u32[]{:S(2)}, u32[]{:S(2)}) collective-permute-start(bf16[1408,128]{1,0:T(8,128)(2,1)S(1)} %collective-permute-done.7), channel_id=1, source_target_pairs={{0,2},{2,4},{4,6},{6,8},{8,10},{10,12},{12,14},{14,16},{16,18},{18... | collective-permute-start | bytes 1081352 | tf_op jit(solution)/shard_map/ppermute | solution.py:57
  459.5 0.8 copy-start.20
  460.3 12.4 %collective-permute-start.9 = (bf16[1408,128]{1,0:T(8,128)(2,1)S(1)}, bf16[1408,128]{1,0:T(8,128)(2,1)S(1)}, u32[]{:S(2)}, u32[]{:S(2)}) collective-permute-start(bf16[1408,128]{1,0:T(8,128)(2,1)S(1)} %collective-permute-done.8), channel_id=1, source_target_pairs={{0,2},{2,4},{4,6},{6,8},{8,10},{10,12},{12,14},{14,16},{16,18},{18... | collective-permute-start | bytes 1081352 | tf_op jit(solution)/shard_map/ppermute | solution.py:57
  472.7 0.8 copy-start.22
  473.4 11.6 %collective-permute-start.10 = (bf16[1408,128]{1,0:T(8,128)(2,1)S(1)}, bf16[1408,128]{1,0:T(8,128)(2,1)}, u32[]{:S(2)}, u32[]{:S(2)}) collective-permute-start(bf16[1408,128]{1,0:T(8,128)(2,1)S(1)} %collective-permute-done.9), channel_id=1, source_target_pairs={{0,2},{2,4},{4,6},{6,8},{8,10},{10,12},{12,14},{14,16},{16,18},{18... | collective-permute-start | bytes 1081352 | tf_op jit(solution)/shard_map/ppermute | solution.py:57
  485.1 11.3 %collective-permute-start.11 = (bf16[1408,128]{1,0:T(8,128)(2,1)}, bf16[1408,128]{1,0:T(8,128)(2,1)}, u32[]{:S(2)}, u32[]{:S(2)}) collective-permute-start(bf16[1408,128]{1,0:T(8,128)(2,1)} %collective-permute-done.10), channel_id=1, source_target_pairs={{0,2},{2,4},{4,6},{6,8},{8,10},{10,12},{12,14},{14,16},{16,18},{18... | collective-permute-start | bytes 1081352 | tf_op jit(solution)/shard_map/ppermute | solution.py:57
  485.1 144.0 %all-reduce.5.cloned.1.call-start = ((), (), s32[]{:S(2)}) async-start(), calls=%async_computation.6 | async-start | bytes 3145728 | tf_op jit(solution)/shard_map/psum | solution.py:62
  496.4 19.3 %collective-permute-start.12 = (bf16[1408,128]{1,0:T(8,128)(2,1)}, bf16[1408,128]{1,0:T(8,128)(2,1)S(1)}, u32[]{:S(2)}, u32[]{:S(2)}) collective-permute-start(bf16[1408,128]{1,0:T(8,128)(2,1)} %collective-permute-done.11), channel_id=1, source_target_pairs={{0,2},{2,4},{4,6},{6,8},{8,10},{10,12},{12,14},{14,16},{16,18},{18... | collective-permute-start | bytes 1081352 | tf_op jit(solution)/shard_map/ppermute | solution.py:57
  515.7 0.7 copy-start.24
  516.4 19.8 %collective-permute-start.13 = (bf16[1408,128]{1,0:T(8,128)(2,1)S(1)}, bf16[1408,128]{1,0:T(8,128)(2,1)}, u32[]{:S(2)}, u32[]{:S(2)}) collective-permute-start(bf16[1408,128]{1,0:T(8,128)(2,1)S(1)} %collective-permute-done.12), channel_id=1, source_target_pairs={{0,2},{2,4},{4,6},{6,8},{8,10},{10,12},{12,14},{14,16},{16,18},{18... | collective-permute-start | bytes 1081352 | tf_op jit(solution)/shard_map/ppermute | solution.py:57
  536.3 14.5 %collective-permute-start.14 = (bf16[1408,128]{1,0:T(8,128)(2,1)}, bf16[1408,128]{1,0:T(8,128)(2,1)}, u32[]{:S(2)}, u32[]{:S(2)}) collective-permute-start(bf16[1408,128]{1,0:T(8,128)(2,1)} %collective-permute-done.13), channel_id=1, source_target_pairs={{0,2},{2,4},{4,6},{6,8},{8,10},{10,12},{12,14},{14,16},{16,18},{18... | collective-permute-start | bytes 1081352 | tf_op jit(solution)/shard_map/ppermute | solution.py:57
  536.3 29.2 %copy-start.17 = (bf16[1408,128]{1,0:T(8,128)(2,1)S(1)}, bf16[1408,128]{1,0:T(8,128)(2,1)}, u32[]{:S(2)}) copy-start(bf16[1408,128]{1,0:T(8,128)(2,1)} %copy-done.16) | copy-start | bytes 1081348
  536.3 30.0 %copy-start.15 = (bf16[1408,128]{1,0:T(8,128)(2,1)S(1)}, bf16[1408,128]{1,0:T(8,128)(2,1)}, u32[]{:S(2)}) copy-start(bf16[1408,128]{1,0:T(8,128)(2,1)} %copy-done.14) | copy-start | bytes 1081348
  536.3 30.8 %copy-start.13 = (bf16[1408,128]{1,0:T(8,128)(2,1)S(1)}, bf16[1408,128]{1,0:T(8,128)(2,1)}, u32[]{:S(2)}) copy-start(bf16[1408,128]{1,0:T(8,128)(2,1)} %copy-done.12) | copy-start | bytes 1081348
  554.5 21.3 %copy-start.25 = (bf16[1408,128]{1,0:T(8,128)(2,1)S(1)}, bf16[1408,128]{1,0:T(8,128)(2,1)}, u32[]{:S(2)}) copy-start(bf16[1408,128]{1,0:T(8,128)(2,1)} %copy-done.24) | copy-start | bytes 1081348
  559.9 20.2 %copy-start.23 = (bf16[1408,128]{1,0:T(8,128)(2,1)S(1)}, bf16[1408,128]{1,0:T(8,128)(2,1)}, u32[]{:S(2)}) copy-start(bf16[1408,128]{1,0:T(8,128)(2,1)} %copy-done.22) | copy-start | bytes 1081348
  561.8 19.2 %copy-start.21 = (bf16[1408,128]{1,0:T(8,128)(2,1)S(1)}, bf16[1408,128]{1,0:T(8,128)(2,1)}, u32[]{:S(2)}) copy-start(bf16[1408,128]{1,0:T(8,128)(2,1)} %copy-done.20) | copy-start | bytes 1081348
  563.6 18.2 %copy-start.19 = (bf16[1408,128]{1,0:T(8,128)(2,1)S(1)}, bf16[1408,128]{1,0:T(8,128)(2,1)}, u32[]{:S(2)}) copy-start(bf16[1408,128]{1,0:T(8,128)(2,1)} %copy-done.18) | copy-start | bytes 1081348
  572.0 13.1 %copy-start.11 = (bf16[1408,128]{1,0:T(8,128)(2,1)S(1)}, bf16[1408,128]{1,0:T(8,128)(2,1)}, u32[]{:S(2)}) copy-start(bf16[1408,128]{1,0:T(8,128)(2,1)} %copy-done.10) | copy-start | bytes 1081348
  572.0 13.9 %copy-start.9 = (bf16[1408,128]{1,0:T(8,128)(2,1)S(1)}, bf16[1408,128]{1,0:T(8,128)(2,1)}, u32[]{:S(2)}) copy-start(bf16[1408,128]{1,0:T(8,128)(2,1)} %copy-done.8) | copy-start | bytes 1081348
  572.0 14.7 %copy-start.7 = (bf16[1408,128]{1,0:T(8,128)(2,1)S(1)}, bf16[1408,128]{1,0:T(8,128)(2,1)}, u32[]{:S(2)}) copy-start(bf16[1408,128]{1,0:T(8,128)(2,1)} %copy-done.6) | copy-start | bytes 1081348
  572.0 15.5 %copy-start.5 = (bf16[1408,128]{1,0:T(8,128)(2,1)S(1)}, bf16[1408,128]{1,0:T(8,128)(2,1)}, u32[]{:S(2)}) copy-start(bf16[1408,128]{1,0:T(8,128)(2,1)} %copy-done.4) | copy-start | bytes 1081348
  572.0 17.1 %copy-start.1 = (bf16[384,2048]{1,0:T(8,128)(2,1)S(1)}, bf16[384,2048]{1,0:T(8,128)(2,1)}, u32[]{:S(2)}) copy-start(bf16[384,2048]{1,0:T(8,128)(2,1)} %param.11) | copy-start | bytes 4718596
  581.8 9.8 %copy-start.26 = (f32[2048]{0:T(1024)S(1)}, f32[2048]{0:T(1024)}, u32[]{:S(2)}) copy-start(f32[2048]{0:T(1024)} %param.16) | copy-start | bytes 24580
  589.2 2.4 copy-start.2
Sparse Core Ops, SparseCore 0:
  10.0 91.4 all-gather.5
  104.2 106.9 all-gather.9
  213.9 86.9 all-gather.7
  312.3 19.0 all-reduce.2
  333.9 112.4 all-gather.11
  485.2 102.4 all-gather.13
  612.9 16.2 all-reduce.4
